TPU v7x, 512 devices: a whole 4x8x8 slice. The times are simulated.
512 devices in a mesh: rep: 2 (over z_hi), fs: 32 (over z_lo, y), tp: 8 (over x, core).
Axes of the slice: x: 4, y: 8, z: 8 (z_hi: 2, z_lo: 4; z = z_hi * 4 + z_lo), core: 2. Of those that a mesh axis runs over, the one named last changes fastest.
Arguments:
- tokens: bfloat16 [32768, 2048], P(('rep', 'fs'), 'tp'), may hold values from -6 to 6
- mix_gain: float32 [2048], replicated, may hold values from 0.1 to 1.9
- query_w: bfloat16 [2048, 2048], P('fs', 'tp'), may hold values from -0.125 to 0.125
- key_w: bfloat16 [2048, 2048], P('fs', 'tp'), may hold values from -0.125 to 0.125
- value_w: bfloat16 [2048, 4096], P('fs', 'tp'), may hold values from -0.125 to 0.125
- head_gain: float32 [8, 512], replicated, may hold values from 0.1 to 1.9
- out_w: bfloat16 [4096, 2048], P('tp', 'fs'), may hold values from -0.09375 to 0.09375
- chan_gain: float32 [2048], replicated, may hold values from 0.1 to 1.9
- up_w: bfloat16 [2048, 4096], P('fs', 'tp'), may hold values from -0.125 to 0.125
- down_w: bfloat16 [4096, 2048], P('tp', 'fs'), may hold values from -0.09375 to 0.09375
Outputs:
- layer_out: bfloat16 [32768, 2048], P(('rep', 'fs'), 'tp')
All inputs are finite; a program needn't handle non-finite values.
Results may differ from a plain program's by a relative error of at most 0.019.
Values may be sent and summed in bfloat16 or wider, within the bound.
A program may use at most 64 MiB of HBM per device.

v0:
```python
import jax
import jax.numpy as jnp
from jax import lax
from jax.sharding import PartitionSpec as P

DK = 256
DV = 512
BLOCK = 128
EPS = 1e-06
HEAD_EPS = 0.05
THETA = 10000.0


def gather_turned(arrays, axis, dims):
    turned = [jnp.moveaxis(a, dim, 0) for a, dim in zip(arrays, dims)]
    both = jnp.concatenate([t.reshape(len(t), -1) for t in turned], axis=1)
    whole, at, finished = (lax.all_gather(both, axis, axis=0, tiled=True), 0, [])
    for t, dim in zip(turned, dims):
        section = whole[:, at : at + t[0].size].reshape(-1, *t.shape[1:])
        finished.append(jnp.moveaxis(section, 0, dim))
        at += t[0].size
    return tuple(finished)


def in_order(blocks, dim):
    shape = list(blocks.shape[1:])
    shape[dim] *= blocks.shape[0]
    return jnp.moveaxis(blocks, 0, dim).reshape(shape)


def copy_for_each(value, axis):
    count = lax.axis_size(axis)
    return lax.all_to_all(
        jnp.broadcast_to(value[None], (count, *value.shape)), axis, 0, 0, tiled=True
    )


def gathered_copies(value, axis, dim):
    return in_order(copy_for_each(value, axis), dim)


def cut_along(value, dim, count):
    shape = value.shape
    blocks = value.reshape(*shape[:dim], count, shape[dim] // count, *shape[dim + 1 :])
    return jnp.moveaxis(blocks, dim, 0)


def sum_at_owner(value, axis, dim):
    count = lax.axis_size(axis)
    blocks = lax.all_to_all(cut_along(value, dim, count), axis, 0, 0, tiled=True)
    return jnp.sum(blocks.astype(jnp.float32), axis=0)


def norm_rows(rows, gain):
    values = rows.astype(jnp.float32)
    scale = lax.rsqrt(jnp.mean(values * values, axis=-1, keepdims=True) + EPS)
    return (values * scale * gain).astype(jnp.bfloat16)


def rotate(field, places):
    half = field.shape[-1] // 2
    inverse = THETA ** (-jnp.arange(half, dtype=jnp.float32) / half)
    angles = places[:, None] * inverse
    cosine = jnp.cos(angles)[:, None, :]
    sine = jnp.sin(angles)[:, None, :]
    first = field[..., :half]
    second = field[..., half:]
    return jnp.concatenate(
        [first * cosine - second * sine, second * cosine + first * sine], axis=-1
    )


def retain(query, keys, values, log_rate):
    count = query.shape[0] // BLOCK
    q_blocks = query.reshape(count, BLOCK, query.shape[1])
    k_blocks = keys.reshape(count, BLOCK, keys.shape[1])
    v_blocks = values.reshape(count, BLOCK, values.shape[1])
    place = jnp.arange(BLOCK, dtype=jnp.float32)
    offset = place[:, None] - place[None, :]
    mask = jnp.where(offset >= 0, jnp.exp(log_rate * jnp.maximum(offset, 0.0)), 0.0)
    q_decay = jnp.exp(log_rate * (place + 1.0))
    k_decay = jnp.exp(log_rate * (BLOCK - 1.0 - place))
    block_decay = jnp.exp(log_rate * BLOCK)

    def advance(state, item):
        q_part, k_part, v_part = item
        scores = jnp.dot(q_part, k_part.T, preferred_element_type=jnp.float32)
        weights = (scores * mask).astype(jnp.bfloat16)
        result = jnp.dot(weights, v_part, preferred_element_type=jnp.float32)
        q_scaled = (q_part.astype(jnp.float32) * q_decay[:, None]).astype(jnp.bfloat16)
        result = result + jnp.dot(
            q_scaled, state.astype(jnp.bfloat16), preferred_element_type=jnp.float32
        )
        k_scaled = (k_part.astype(jnp.float32) * k_decay[:, None]).astype(jnp.bfloat16)
        state = state * block_decay + jnp.dot(
            k_scaled.T, v_part, preferred_element_type=jnp.float32
        )
        return (state, result)

    start = jnp.zeros((query.shape[1], values.shape[1]), jnp.float32)
    _, outputs = lax.scan(advance, start, (q_blocks, k_blocks, v_blocks))
    return outputs.reshape(count * BLOCK, values.shape[1])


def shards(tokens, mix_gain, query_w, key_w, value_w, head_gain, out_w, chan_gain, up_w, down_w):
    rows = tokens.shape[0]
    local = query_w.shape[1] // DK
    query_all, key_all, value_all, out_all, up_all, down_all = gather_turned(
        (query_w, key_w, value_w, out_w, up_w, down_w), "fs", (0, 0, 0, 1, 0, 1)
    )
    whole = gathered_copies(tokens, "tp", 1)
    normed = norm_rows(whole, mix_gain)
    qraw = jnp.dot(normed, query_all, preferred_element_type=jnp.float32)
    kraw = jnp.dot(normed, key_all, preferred_element_type=jnp.float32)
    vraw = jnp.dot(normed, value_all, preferred_element_type=jnp.float32)
    places = jnp.arange(rows, dtype=jnp.int32).astype(jnp.float32)
    query = rotate(qraw.reshape(rows, local, DK), places).astype(jnp.bfloat16)
    keys = (rotate(kraw.reshape(rows, local, DK), places) * DK ** (-0.5)).astype(jnp.bfloat16)
    values = vraw.reshape(rows, local, DV).astype(jnp.bfloat16)
    first_head = lax.axis_index("tp") * local
    heads = (first_head + jnp.arange(local, dtype=jnp.int32)).astype(jnp.float32)
    log_rate = jnp.log1p(-jnp.exp2(-5.0 - heads))
    retained = jax.vmap(retain, in_axes=(1, 1, 1, 0), out_axes=1)(query, keys, values, log_rate)
    gains = lax.dynamic_slice_in_dim(head_gain, first_head, local, 0)
    scale = lax.rsqrt(jnp.mean(retained * retained, axis=-1, keepdims=True) + HEAD_EPS)
    head_out = (retained * scale * gains).astype(jnp.bfloat16).reshape(rows, local * DV)
    mixer_terms = jnp.dot(head_out, out_all, preferred_element_type=jnp.float32)
    mixed = sum_at_owner(mixer_terms.astype(jnp.bfloat16), "tp", 1)
    middle = (tokens.astype(jnp.float32) + mixed).astype(jnp.bfloat16)
    whole_middle = gathered_copies(middle, "tp", 1)
    chan_normed = norm_rows(whole_middle, chan_gain)
    upward = jnp.dot(chan_normed, up_all, preferred_element_type=jnp.float32)
    hidden = jnp.square(jax.nn.relu(upward)).astype(jnp.bfloat16)
    chan_terms = jnp.dot(hidden, down_all, preferred_element_type=jnp.float32)
    channel = sum_at_owner(chan_terms.astype(jnp.bfloat16), "tp", 1)
    return (middle.astype(jnp.float32) + channel).astype(jnp.bfloat16)


def solution(mesh):
    placed = (
        P(("rep", "fs"), "tp"),
        P(),
        P("fs", "tp"),
        P("fs", "tp"),
        P("fs", "tp"),
        P(),
        P("tp", "fs"),
        P(),
        P("fs", "tp"),
        P("tp", "fs"),
    )
    return jax.shard_map(
        shards, mesh=mesh, in_specs=placed, out_specs=P(("rep", "fs"), "tp"), check_vma=False
    )
```

profile of v0, /device:TPU:1, one launch (start us, length us, event | category | flops | bytes accessed | tf_op | source)
XLA Modules:
  0.0 313.0 jit_solution(4496840921103430434)
XLA Ops:
  6.5 0.8 constant_dynamic-update-slice_fusion.3
  7.3 0.8 constant_dynamic-update-slice_fusion.2
  8.1 0.8 constant_dynamic-update-slice_fusion.1
  8.9 0.8 bitcast_dynamic-update-slice_fusion.1
  9.8 0.8 constant_dynamic-update-slice_fusion
  10.6 0.8 bitcast_dynamic-update-slice_fusion
  12.2 1.1 copy.23
  13.3 1.5 broadcast_in_dim.15
  14.8 10.3 %all-to-all-start = ((bf16[8,512,256]{1,2,0:T(8,128)(2,1)}), bf16[8,512,256]{1,2,0:T(8,128)(2,1)S(1)}, u32[]{:S(2)}, u32[]{:S(2)}) async-start(bf16[8,512,256]{1,2,0:T(8,128)(2,1)} %broadcast_in_dim.15), calls=%async_computation | async-start | bytes 4194304 | tf_op jit(solution)/shard_map/all_to_all | solution.py:33
  25.3 26.1 %all-to-all-done = bf16[8,512,256]{1,2,0:T(8,128)(2,1)S(1)} async-done(((bf16[8,512,256]{1,2,0:T(8,128)(2,1)}), bf16[8,512,256]{1,2,0:T(8,128)(2,1)S(1)}, u32[]{:S(2)}, u32[]{:S(2)}) %all-to-all-start) | async-done | bytes 2097184 | tf_op jit(solution)/shard_map/all_to_all | solution.py:33
  52.0 1.9 fusion.57
  53.8 117.0 %all-gather.2.cloned.1.call-done = bf16[2048,2560]{1,0:T(8,128)(2,1)} async-done(((bf16[64,2560]{1,0:T(8,128)(2,1)}), bf16[2048,2560]{1,0:T(8,128)(2,1)}) %all-gather.2.cloned.1.call-update) | async-done | bytes 10485776 | tf_op jit(solution)/shard_map/all_gather | solution.py:17
  170.9 2.6 convolution_bitcast_fusion.2
  173.5 2.0 convolution_bitcast_fusion.1
  175.5 1.2 fusion.95
  177.0 3.0 fusion.70
  180.0 3.8 %while.15 = (s32[]{:T(128)}, f32[1,256,512]{2,1,0:T(8,128)S(1)}, f32[4,1,128,512]{3,2,1,0:T(8,128)S(1)}, f32[1]{0:T(128)}, bf16[4,1,128,256]{3,2,1,0:T(8,128)(2,...) while((s32[]{:T(128)}, f32[1,256,512]{2,1,0:T(8,128)S(1)}, ...), condition=%wide.region_2.3_spmd.clone.clone.clone, body=%wide.region_1.2_spmd.clone.clone.clone.sunk | while | flops 93176320 | bytes 2890356 | solution.py:101
  184.2 2.9 convolution_convert_fusion.1
  187.2 49.3 %all_to_all.20 = bf16[8,512,256]{2,1,0:T(8,128)(2,1)S(1)} all-to-all(bf16[8,512,256]{2,1,0:T(8,128)(2,1)S(1)} %bitcast.148), channel_id=1, replica_groups=mesh['rep'=2,'fs'=32,'tp'=8] {'tp'}, dimensions={0} | all-to-all | bytes 4194304 | tf_op jit(solution)/shard_map/all_to_all | solution.py:50
  237.8 29.7 %all_to_all.21 = bf16[8,512,256]{1,2,0:T(8,128)(2,1)S(1)} all-to-all(bf16[8,512,256]{1,2,0:T(8,128)(2,1)S(1)} %broadcast_in_dim.16), channel_id=1, replica_groups=mesh['rep'=2,'fs'=32,'tp'=8] {'tp'}, dimensions={0} | all-to-all | bytes 4194304 | tf_op jit(solution)/shard_map/all_to_all | solution.py:33
  268.2 1.9 fusion.55
  270.0 5.2 %convolution_convert_fusion = bf16[512,2048]{1,0:T(8,128)(2,1)S(1)} fusion(bf16[2048,2560]{1,0:T(8,128)(2,1)} %all-gather.2.cloned.1.call-done, bf16[512,2048]{0,1:T(8,128)(2,1)} %fusion.55), kind=kOutput, calls=%fused_computation.61 | convolution fusion | flops 2149318656 | bytes 8388608 | tf_op jit(solution)/shard_map/dot_general | solution.py:134
  275.4 29.7 %all_to_all.22 = bf16[8,512,256]{2,1,0:T(8,128)(2,1)S(1)} all-to-all(bf16[8,512,256]{2,1,0:T(8,128)(2,1)S(1)} %bitcast.149), channel_id=1, replica_groups=mesh['rep'=2,'fs'=32,'tp'=8] {'tp'}, dimensions={0} | all-to-all | bytes 4194304 | tf_op jit(solution)/shard_map/all_to_all | solution.py:50
  305.4 0.8 add_convert_fusion
  (55 shorter events, 8.1 us)
Async XLA Ops:
  6.5 18.7 %copy-start = (f32[8,512]{1,0:T(8,128)S(1)}, f32[8,512]{1,0:T(8,128)}, u32[]{:S(2)}) copy-start(f32[8,512]{1,0:T(8,128)} %param.17) | copy-start | bytes 49156
  6.5 164.3 %all-gather.2.cloned.1.call-start = ((), (), s32[]{:S(2)}) async-start(), calls=%async_computation.4 | async-start | bytes 10813440 | tf_op jit(solution)/shard_map/all_gather | solution.py:17
  11.4 0.7 copy-start.5
  14.8 36.7 %all-to-all-start = ((bf16[8,512,256]{1,2,0:T(8,128)(2,1)}), bf16[8,512,256]{1,2,0:T(8,128)(2,1)S(1)}, u32[]{:S(2)}, u32[]{:S(2)}) async-start(bf16[8,512,256]{1,2,0:T(8,128)(2,1)} %broadcast_in_dim.15), calls=%async_computation | async-start | bytes 4194304 | tf_op jit(solution)/shard_map/all_to_all | solution.py:33
  25.1 26.9 %copy-start.6 = (f32[2048]{0:T(1024)S(1)}, f32[2048]{0:T(1024)}, u32[]{:S(2)}) copy-start(f32[2048]{0:T(1024)} %param.13) | copy-start | bytes 24580
  53.8 119.6 %copy-start.2 = (bf16[512,2048]{0,1:T(8,128)(2,1)S(1)}, bf16[512,2048]{0,1:T(8,128)(2,1)}, u32[]{:S(2)}) copy-start(bf16[512,2048]{0,1:T(8,128)(2,1)} %fusion.57) | copy-start | bytes 6291460
  175.5 1.6 copy-start.3
  177.0 3.0 copy-start.1
  236.5 1.0 copy-start.4
  267.5 0.7 copy-start.7
Sparse Core Ops, SparseCore 0:
  12.3 158.5 all-gather.1
where the time goes:
time: 314 us; the launch traced here: 313 us
  waiting for transfers between devices  143 us (46%)
  blocking collectives  109 us (35%)
  matrix products  19.2 us (6%)
  between operations  13.7 us (4%)
  starting transfers between devices  10.3 us (3%)
  local copies, waits for them, and re-layouts  9.88 us (3%)
  other arithmetic  7.86 us (3%)
    all_gather x1, waiting for transfers between devices, gather_turned(): lax.all_gather(both, axis, axis=0, tiled=True)  117 us
    all_to_all x2, blocking collectives, sum_at_owner(): lax.all_to_all(cut_along(value, dim, count), axis, 0, 0, tiled=True)  78.9 us
    all_to_all x1, blocking collectives, copy_for_each(): lax.all_to_all(jnp.broadcast_to(value[None], (count, *value.shape)), axis...  29.7 us
    all_to_all x1, waiting for transfers between devices, copy_for_each(): lax.all_to_all(jnp.broadcast_to(value[None], (count, *value.shape)), axis...  26.1 us
    all_to_all x1, starting transfers between devices, copy_for_each(): lax.all_to_all(jnp.broadcast_to(value[None], (count, *value.shape)), axis...  10.3 us
    unnamed x22, local copies, waits for them, and re-layouts  6.96 us
  transfers between devices with their start and end apart: 2, of which 2 were waited for; matrix products, arithmetic and copies ran while one was open for 2% of the time, Pallas kernels for 0%

commit v1 on v0

--- a/solution.py
+++ b/solution.py
@@ -14,7 +14,13 @@
 def gather_turned(arrays, axis, dims):
     turned = [jnp.moveaxis(a, dim, 0) for a, dim in zip(arrays, dims)]
     both = jnp.concatenate([t.reshape(len(t), -1) for t in turned], axis=1)
-    whole, at, finished = (lax.all_gather(both, axis, axis=0, tiled=True), 0, [])
+    whole, at, finished = (
+        jnp.concatenate(
+            lax.all_to_all(jnp.stack([both] * lax.axis_size(axis)), axis, 0, 0), axis=0
+        ),
+        0,
+        [],
+    )
     for t, dim in zip(turned, dims):
         section = whole[:, at : at + t[0].size].reshape(-1, *t.shape[1:])
         finished.append(jnp.moveaxis(section, 0, dim))

time: 314 us -> 484 us (1.54)
  the two profiles are of different devices: /device:TPU:1 before, /device:TPU:120 now
where the time goes in v1:
time: 484 us; the launch traced here: 483 us
  waiting for transfers between devices  341 us (70%)
  blocking collectives  89 us (18%)
  matrix products  19.2 us (4%)
  starting transfers between devices  16 us (3%)
  local copies, waits for them, and re-layouts  9.12 us (2%)
  other arithmetic  7.88 us (2%)
    all_to_all x1, waiting for transfers between devices, gather_turned(): lax.all_to_all(jnp.stack([both] * lax.axis_size(axis)), axis, 0, 0)  314 us
    all_to_all x2, blocking collectives, sum_at_owner(): lax.all_to_all(cut_along(value, dim, count), axis, 0, 0, tiled=True)  59.3 us
    all_to_all x1, blocking collectives, copy_for_each(): lax.all_to_all(jnp.broadcast_to(value[None], (count, *value.shape)), axis...  29.7 us
    all_to_all x1, waiting for transfers between devices, copy_for_each(): lax.all_to_all(jnp.broadcast_to(value[None], (count, *value.shape)), axis...  27 us
    all_to_all x1, starting transfers between devices, gather_turned(): lax.all_to_all(jnp.stack([both] * lax.axis_size(axis)), axis, 0, 0)  11.6 us
  transfers between devices with their start and end apart: 2, of which 2 were waited for; matrix products, arithmetic and copies ran while one was open for 1% of the time, Pallas kernels for 0%

profile of v1, /device:TPU:120, one launch (start us, length us, event | category | flops | bytes accessed | tf_op | source)
XLA Modules:
  0.0 483.1 jit_solution(8598965904112530689)
XLA Ops:
  0.0 1.1 copy.23
  1.1 1.5 broadcast_in_dim.15
  2.7 4.4 all-to-all-start
  7.2 27.0 %all-to-all-done = bf16[8,512,256]{1,2,0:T(8,128)(2,1)S(1)} async-done(((bf16[8,512,256]{1,2,0:T(8,128)(2,1)}), bf16[8,512,256]{1,2,0:T(8,128)(2,1)S(1)}, u32[]{:S(2)}, u32[]{:S(2)}) %all-to-all-start) | async-done | bytes 2097184 | tf_op jit(solution)/shard_map/all_to_all | solution.py:39
  34.3 5.0 %stack.2 = bf16[32,64,2560]{2,1,0:T(8,128)(2,1)} broadcast(bf16[64,2560]{1,0:T(8,128)(2,1)S(1)} %bitcast_dynamic-update-slice_fusion), dimensions={1,2} | broadcast | bytes 10813440 | tf_op jit(solution)/shard_map/stack | solution.py:19
  39.3 11.6 %all-to-all-start.1 = ((bf16[32,64,2560]{2,1,0:T(8,128)(2,1)}), bf16[32,64,2560]{2,1,0:T(8,128)(2,1)}, u32[]{:S(2)}, u32[]{:S(2)}) async-start(bf16[32,64,2560]{2,1,0:T(8,128)(2,1)} %stack.2), calls=%async_computation.1 | async-start | bytes 20971520 | tf_op jit(solution)/shard_map/all_to_all | solution.py:19
  51.1 0.5 multiply_reduce_fusion.1
  51.6 1.9 fusion.57
  53.5 314.2 %all-to-all-done.1 = bf16[32,64,2560]{2,1,0:T(8,128)(2,1)} async-done(((bf16[32,64,2560]{2,1,0:T(8,128)(2,1)}), bf16[32,64,2560]{2,1,0:T(8,128)(2,1)}, u32[]{:S(2)}, u32[]{:S(2)}) %all-to-all-start.1) | async-done | bytes 10485792 | tf_op jit(solution)/shard_map/all_to_all | solution.py:19
  367.7 2.7 convolution_bitcast_fusion.2
  370.5 2.0 convolution_bitcast_fusion.1
  372.4 2.9 fusion.70
  375.3 1.2 fusion.95
  376.7 3.8 while.15
  376.7 0.3 fusion.122
  380.8 2.9 convolution_convert_fusion.1
  383.8 29.7 %all_to_all.25 = bf16[8,512,256]{2,1,0:T(8,128)(2,1)S(1)} all-to-all(bf16[8,512,256]{2,1,0:T(8,128)(2,1)S(1)} %bitcast.149), channel_id=1, replica_groups=mesh['rep'=2,'fs'=32,'tp'=8] {'tp'}, dimensions={0} | all-to-all | bytes 4194304 | tf_op jit(solution)/shard_map/all_to_all | solution.py:56
  413.8 0.6 copy-done.3
  414.8 29.7 %all_to_all.26 = bf16[8,512,256]{1,2,0:T(8,128)(2,1)S(1)} all-to-all(bf16[8,512,256]{1,2,0:T(8,128)(2,1)S(1)} %broadcast_in_dim.16), channel_id=1, replica_groups=mesh['rep'=2,'fs'=32,'tp'=8] {'tp'}, dimensions={0} | all-to-all | bytes 4194304 | tf_op jit(solution)/shard_map/all_to_all | solution.py:39
  444.5 0.5 multiply_reduce_fusion
  445.2 1.9 fusion.55
  447.0 5.2 %convolution_convert_fusion = bf16[512,2048]{1,0:T(8,128)(2,1)S(1)} fusion(bf16[2048,2560]{1,0:T(8,128)(2,1)} %bitcast.5, bf16[512,2048]{0,1:T(8,128)(2,1)} %fusion.55), kind=kOutput, calls=%fused_computation.61 | convolution fusion | flops 2149318656 | bytes 8388608 | tf_op jit(solution)/shard_map/dot_general | solution.py:140
  452.4 29.7 %all_to_all.27 = bf16[8,512,256]{2,1,0:T(8,128)(2,1)S(1)} all-to-all(bf16[8,512,256]{2,1,0:T(8,128)(2,1)S(1)} %bitcast.150), channel_id=1, replica_groups=mesh['rep'=2,'fs'=32,'tp'=8] {'tp'}, dimensions={0} | all-to-all | bytes 4194304 | tf_op jit(solution)/shard_map/all_to_all | solution.py:56
  482.4 0.8 add_convert_fusion
  (63 shorter events, 5.2 us)
Async XLA Ops:
  0.0 51.1 %copy-start = (f32[8,512]{1,0:T(8,128)S(1)}, f32[8,512]{1,0:T(8,128)}, u32[]{:S(2)}) copy-start(f32[8,512]{1,0:T(8,128)} %param.17) | copy-start | bytes 49156
  2.6 4.5 copy-start.8
  2.6 4.5 copy-start.9
  2.6 4.5 copy-start.4
  2.6 4.5 copy-start.5
  2.6 4.6 copy-start.6
  2.6 4.6 copy-start.7
  2.7 31.6 %all-to-all-start = ((bf16[8,512,256]{1,2,0:T(8,128)(2,1)}), bf16[8,512,256]{1,2,0:T(8,128)(2,1)S(1)}, u32[]{:S(2)}, u32[]{:S(2)}) async-start(bf16[8,512,256]{1,2,0:T(8,128)(2,1)} %broadcast_in_dim.15), calls=%async_computation | async-start | bytes 4194304 | tf_op jit(solution)/shard_map/all_to_all | solution.py:39
  39.3 328.4 %all-to-all-start.1 = ((bf16[32,64,2560]{2,1,0:T(8,128)(2,1)}), bf16[32,64,2560]{2,1,0:T(8,128)(2,1)}, u32[]{:S(2)}, u32[]{:S(2)}) async-start(bf16[32,64,2560]{2,1,0:T(8,128)(2,1)} %stack.2), calls=%async_computation.1 | async-start | bytes 20971520 | tf_op jit(solution)/shard_map/all_to_all | solution.py:19
  50.9 0.7 copy-start.10
  367.7 2.8 copy-start.2
  375.3 1.3 copy-start.1
  413.5 1.0 copy-start.3
  444.5 0.7 copy-start.11
